TPU v7x, 32 devices: a whole 2x2x4 slice. The times are simulated.
32 devices in a mesh: sp: 16 (over z, y, x), tp: 2 (over core).
Axes of the slice: x: 2, y: 2, z: 4, core: 2. Of those that a mesh axis runs over, the one named last changes fastest.
Arguments:
- residual: bfloat16 [2048, 4096], P('tp', 'sp'), may hold values from -6 to 6
- values: bfloat16 [4096, 4096], P('sp', 'tp'), may hold values from -6 to 6
- gate_input: bfloat16 [4096, 4096], P('sp', 'tp'), may hold values from -6 to 6
- group_keys: bfloat16 [4096, 3072], P('sp', 'tp'), may hold values from -6 to 6
- time_step: float32 [64, 4096], P('tp', 'sp'), may hold values from -8 to 14
- decay_rate: float32 [64], P('tp'), may hold values from 0 to 2
- skip_gain: float32 [64], P('tp'), may hold values from 0.25 to 2
- conv_values: bfloat16 [4, 4096], P(None, 'tp'), may hold values from -3 to 3
- conv_keys: bfloat16 [4, 3072], P(None, 'tp'), may hold values from -3 to 3
- mix_gain: float32 [4096], P('tp'), may hold values from 0.1 to 1.9
- out_weight: bfloat16 [4096, 2048], P('tp'), may hold values from -0.09375 to 0.09375
- norm_gain: float32 [2048], replicated, may hold values from 0.1 to 1.9
- hidden_gate: bfloat16 [2048, 5120], P('sp', 'tp'), may hold values from -0.125 to 0.125
- hidden_up: bfloat16 [2048, 5120], P('sp', 'tp'), may hold values from -0.125 to 0.125
- hidden_conv: bfloat16 [2, 3, 5120], P(None, None, 'tp'), may hold values from -3.5 to 3.5
- hidden_down: bfloat16 [5120, 2048], P('tp', 'sp'), may hold values from -0.078125 to 0.078125
Outputs:
- layer_out: bfloat16 [2048, 4096], P('tp', 'sp')
All inputs are finite; a program needn't handle non-finite values.
Results may differ from a plain program's by a relative error of at most 0.019.
Values may be sent and summed in bfloat16 or wider, within the bound.
A program may use at most 128 MiB of HBM per device.

v0:
```python
import jax
import jax.numpy as jnp
from jax import lax
from jax.sharding import PartitionSpec as P

GROUP_HEADS = 8
HEAD_SIZE = 64
STATE_WIDE = 128
STATE_NARROW = 64
BLOCK = 128
NORM_FLOOR = 0.1
HIGHEST = lax.Precision.HIGHEST


def from_behind(value, axis, steps):
    count = lax.axis_size(axis)
    first, last = (max(0, -steps), min(count, count - steps))
    return lax.ppermute(value, axis, [(source, source + steps) for source in range(first, last)])


def prefix(shard, axis, join, neutral):
    place = lax.axis_index(axis)
    gathered = jax.tree.map(
        lambda a, kind: lax.all_gather(a.astype(kind), axis),
        shard,
        (jnp.bfloat16, jnp.bfloat16, jnp.bfloat16, jnp.bfloat16),
    )
    state = jax.tree.map(lambda a, e: jnp.zeros_like(a) + jnp.asarray(e, a.dtype), shard, neutral)

    def one(lap, state):
        return join(
            state,
            jax.tree.map(
                lambda a, own: lax.dynamic_index_in_dim(a, lap, 0, False).astype(own.dtype),
                gathered,
                shard,
            ),
        )

    return lax.fori_loop(0, place, one, state)


def from_partner_2(shard, axis, stride):
    return lax.ppermute(shard, axis, [(i, i ^ 1 << stride) for i in range(lax.axis_size(axis))])


def tap_sum(joined, weights, row_count):
    summed = weights[0].astype(jnp.float32) * joined[0:row_count]
    for tap_index in range(1, weights.shape[0]):
        summed = (
            summed
            + weights[tap_index].astype(jnp.float32) * joined[tap_index : tap_index + row_count]
        )
    return summed


def block_heads(inputs, in_keys, out_keys, deltas, decay_rates, skip_table, carried):
    length = inputs.shape[0]
    running = jnp.cumsum(-decay_rates * deltas, axis=0)
    weighted = inputs * deltas[..., None]
    scores = jnp.einsum("ign,jgn->gij", out_keys, in_keys, precision=HIGHEST)
    by_head = jnp.transpose(running, (1, 2, 0))
    between = by_head[..., :, None] - by_head[..., None, :]
    lower_mask = jnp.tril(jnp.ones((length, length), dtype=bool))
    decays = jnp.exp(jnp.where(lower_mask, between, -jnp.inf))
    inside = jnp.einsum("ghij,jghp->ighp", scores[:, None] * decays, weighted, precision=HIGHEST)
    carried_part = (
        jnp.einsum("ign,ghpn->ighp", out_keys, carried, precision=HIGHEST)
        * jnp.exp(running)[..., None]
    )
    to_end = jnp.exp(by_head[..., -1:] - by_head)
    fresh_state = jnp.einsum("jgn,ghj,jghp->ghpn", in_keys, to_end, weighted, precision=HIGHEST)
    updated = carried * jnp.exp(by_head[..., -1])[..., None, None] + fresh_state
    return (inside + carried_part + inputs * skip_table[..., None], updated)


def contract_rows(left, right):
    return lax.dot_general(
        left, right, (((0,), (0,)), ((), ())), preferred_element_type=jnp.float32
    )


def combine_states(first_part, second_part):
    return (
        first_part[0] * second_part[0],
        first_part[1] * second_part[0][..., None, None] + second_part[1],
        first_part[2] * second_part[2],
        first_part[3] * second_part[2][..., None, None] + second_part[3],
    )


def hidden_taps(both_pre, edge_cols, taps, row_count):
    joined_hidden = jnp.concatenate([edge_cols, both_pre], axis=2).astype(jnp.float32)
    conv_total = taps[:, 0, :, None].astype(jnp.float32) * joined_hidden[:, :, 0:row_count]
    for tap_index in range(1, taps.shape[1]):
        conv_total = (
            conv_total
            + taps[:, tap_index, :, None].astype(jnp.float32)
            * joined_hidden[:, :, tap_index : tap_index + row_count]
        )
    return (jax.nn.silu(conv_total[0]) * conv_total[1]).astype(jnp.bfloat16)


def local(
    residual,
    values,
    gate_input,
    group_keys,
    time_step,
    decay_rate,
    skip_gain,
    conv_values,
    conv_keys,
    mix_gain,
    out_weight,
    norm_gain,
    hidden_gate,
    hidden_up,
    hidden_conv,
    hidden_down,
):
    row_count = values.shape[0]
    value_cols = values.shape[1]
    tap_count = conv_values.shape[0]
    tail_rows = jnp.concatenate(
        [values[row_count - tap_count + 1 :], group_keys[row_count - tap_count + 1 :]], axis=1
    )
    before_rows = from_behind(tail_rows, "sp", 1)
    joined_values = jnp.concatenate([before_rows[:, :value_cols], values], axis=0).astype(
        jnp.float32
    )
    joined_keys = jnp.concatenate([before_rows[:, value_cols:], group_keys], axis=0).astype(
        jnp.float32
    )
    group_count = group_keys.shape[1] // (2 * STATE_WIDE + 2 * STATE_NARROW)
    inputs = jax.nn.silu(tap_sum(joined_values, conv_values, row_count)).reshape(
        row_count, group_count, GROUP_HEADS, HEAD_SIZE
    )
    key_rows = jax.nn.silu(tap_sum(joined_keys, conv_keys, row_count)).reshape(
        row_count, group_count, -1
    )
    deltas = jax.nn.softplus(time_step).T.reshape(row_count, group_count, GROUP_HEADS)
    rate_table = decay_rate.reshape(group_count, GROUP_HEADS)
    skip_table = skip_gain.reshape(group_count, GROUP_HEADS)
    running = jnp.cumsum(-rate_table * deltas, axis=0)
    half_heads = GROUP_HEADS // 2
    wide_end = 2 * STATE_WIDE

    def run_kind(head_first, head_last, key_first, state_width):
        in_keys = key_rows[..., key_first : key_first + state_width]
        out_keys = key_rows[..., key_first + state_width : key_first + 2 * state_width]
        carried = jnp.zeros(
            (group_count, head_last - head_first, HEAD_SIZE, state_width), jnp.float32
        )
        block_outs = []
        for block_index in range(row_count // BLOCK):
            row_first = block_index * BLOCK
            row_last = row_first + BLOCK
            block_out, carried = block_heads(
                inputs[row_first:row_last, :, head_first:head_last],
                in_keys[row_first:row_last],
                out_keys[row_first:row_last],
                deltas[row_first:row_last, :, head_first:head_last],
                rate_table[:, head_first:head_last],
                skip_table[:, head_first:head_last],
                carried,
            )
            block_outs.append(block_out)
        return (jnp.concatenate(block_outs, axis=0), carried, out_keys)

    wide_local, wide_state, wide_keys = run_kind(0, half_heads, 0, STATE_WIDE)
    narrow_local, narrow_state, narrow_keys = run_kind(
        half_heads, GROUP_HEADS, wide_end, STATE_NARROW
    )
    span_decay = jnp.exp(running[-1])
    start_value = (
        jnp.ones_like(span_decay[:, :half_heads]),
        jnp.zeros_like(wide_state),
        jnp.ones_like(span_decay[:, half_heads:]),
        jnp.zeros_like(narrow_state),
    )
    incoming = prefix(
        (span_decay[:, :half_heads], wide_state, span_decay[:, half_heads:], narrow_state),
        "sp",
        combine_states,
        start_value,
    )
    growth = jnp.exp(running)[..., None]
    wide_out = (
        wide_local
        + jnp.einsum("ign,ghpn->ighp", wide_keys, incoming[1], precision=HIGHEST)
        * growth[:, :, :half_heads]
    )
    narrow_out = (
        narrow_local
        + jnp.einsum("ign,ghpn->ighp", narrow_keys, incoming[3], precision=HIGHEST)
        * growth[:, :, half_heads:]
    )
    mixer_out = jnp.concatenate([wide_out, narrow_out], axis=2).reshape(row_count, value_cols)
    gated_out = mixer_out * jax.nn.silu(gate_input.astype(jnp.float32))
    squares = lax.psum(jnp.sum(gated_out * gated_out, axis=1), "tp")
    inverse_rms = lax.rsqrt(squares / (value_cols * lax.axis_size("tp")) + NORM_FLOOR)
    normed = (gated_out * inverse_rms[:, None] * mix_gain).astype(jnp.bfloat16)
    mixer_sum = lax.psum_scatter(
        lax.dot_general(
            out_weight, normed, (((0,), (1,)), ((), ())), preferred_element_type=jnp.float32
        ).astype(jnp.bfloat16),
        "tp",
        scatter_dimension=0,
        tiled=True,
    ).astype(jnp.float32)
    own_merged = (residual.astype(jnp.float32) + mixer_sum).astype(jnp.bfloat16)
    merged = lax.all_gather(own_merged, "tp", axis=0, tiled=True)
    merged_wide = merged.astype(jnp.float32)
    inverse_norm = lax.rsqrt(jnp.mean(merged_wide * merged_wide, axis=0) + NORM_FLOOR)
    lifted = (merged_wide * inverse_norm[None, :] * norm_gain[:, None]).astype(jnp.bfloat16)
    hidden_cols = hidden_gate.shape[1]
    edge_taps = hidden_conv.shape[1]
    half_cols = hidden_cols // 2
    parity = lax.axis_index("sp") % 2
    first_member = parity == 0
    sp_count = lax.axis_size("sp")
    weight_rows = hidden_gate.shape[0]
    gate_tiles = jnp.tile(
        jnp.stack([hidden_gate[:, :half_cols], hidden_gate[:, half_cols:]]), (sp_count // 2, 1, 1)
    )
    up_tiles = jnp.tile(
        jnp.stack([hidden_up[:, :half_cols], hidden_up[:, half_cols:]]), (sp_count // 2, 1, 1)
    )
    gate_half, up_half = (
        lax.all_to_all(gate_tiles, "sp", split_axis=0, concat_axis=0, tiled=True),
        lax.all_to_all(up_tiles, "sp", split_axis=0, concat_axis=0, tiled=True),
    )
    gate_half = gate_half.reshape(sp_count * weight_rows, half_cols)
    up_half = up_half.reshape(sp_count * weight_rows, half_cols)
    partner_lifted = from_partner_2(lifted, "sp", 0)
    pair_lifted = jnp.where(
        first_member,
        jnp.concatenate([lifted, partner_lifted], axis=1),
        jnp.concatenate([partner_lifted, lifted], axis=1),
    )
    pair_count = 2 * row_count
    pair_pre = jnp.stack(
        [contract_rows(gate_half, pair_lifted), contract_rows(up_half, pair_lifted)]
    ).astype(jnp.bfloat16)
    pair_edge = from_behind(pair_pre[:, :, pair_count - edge_taps + 1 :], "sp", 2)
    half_taps = lax.dynamic_slice_in_dim(hidden_conv, parity * half_cols, half_cols, 2)
    half_hidden = hidden_taps(pair_pre, pair_edge, half_taps, pair_count)
    own_part = lax.dynamic_slice_in_dim(half_hidden, parity * row_count, row_count, 1)
    for_partner = lax.dynamic_slice_in_dim(half_hidden, (1 - parity) * row_count, row_count, 1)
    from_partner = from_partner_2(for_partner, "sp", 0)
    hidden = jnp.where(
        first_member,
        jnp.concatenate([own_part, from_partner], axis=0),
        jnp.concatenate([from_partner, own_part], axis=0),
    )
    down_whole = lax.all_gather(hidden_down, "sp", axis=1, tiled=True)
    hidden_sum = lax.psum_scatter(
        contract_rows(down_whole, hidden).astype(jnp.bfloat16),
        "tp",
        scatter_dimension=0,
        tiled=True,
    ).astype(jnp.float32)
    return (own_merged.astype(jnp.float32) + hidden_sum).astype(jnp.bfloat16)


def solution(mesh):
    in_specs = (
        P("tp", "sp"),
        P("sp", "tp"),
        P("sp", "tp"),
        P("sp", "tp"),
        P("tp", "sp"),
        P("tp"),
        P("tp"),
        P(None, "tp"),
        P(None, "tp"),
        P("tp"),
        P("tp", None),
        P(),
        P("sp", "tp"),
        P("sp", "tp"),
        P(None, None, "tp"),
        P("tp", "sp"),
    )
    out_specs = P("tp", "sp")
    return jax.shard_map(local, mesh=mesh, in_specs=in_specs, out_specs=out_specs, check_vma=False)
```

profile of v0, /device:TPU:0, one launch (start us, length us, event | category | flops | bytes accessed | tf_op | source)
XLA Modules:
  0.0 622.7 jit_solution(8149238865578526616)
XLA Ops:
  8.2 4.9 collective-permute-start
  15.7 1.2 copy.125
  17.7 1.2 divide_multiply_fusion
  19.0 1.9 copy.123
  20.9 1.6 maximum_convert_fusion.1
  22.5 2.4 divide_multiply_fusion.1
  25.5 1.3 fusion.44
  28.5 1.7 convolution_add_fusion.3
  30.2 2.5 fusion.43
  32.7 1.1 slice_bitcast_fusion.7
  33.9 2.8 tile.8
  36.6 6.0 all-to-all-start
  42.7 1.8 exp.125
  44.5 1.0 copy.135
  47.6 2.3 reduce-window.6
  50.1 1.0 copy.138
  51.3 1.1 copy.152
  52.9 125.0 %all-gather.4 = bf16[16,4,4]{2,1,0:T(4,128)(2,1)S(1)} all-gather(bf16[1,4,4]{2,1,0:T(4,128)(2,1)S(1)} %get-tuple-element.151), channel_id=2, replica_groups=mesh['sp'=16,'tp'=2] {'sp'}, dimensions={0}, use_global_device_ids=true | all-gather | bytes 544 | tf_op jit(solution)/shard_map/all_gather | solution.py:24
  177.9 77.3 %all-gather.5 = bf16[16,4,4]{2,1,0:T(4,128)(2,1)S(1)} all-gather(bf16[1,4,4]{2,1,0:T(4,128)(2,1)S(1)} %get-tuple-element.150), channel_id=4, replica_groups=mesh['sp'=16,'tp'=2] {'sp'}, dimensions={0}, use_global_device_ids=true | all-gather | bytes 544 | tf_op jit(solution)/shard_map/all_gather | solution.py:24
  260.1 2.2 fusion.36
  262.3 3.0 fusion.38
  265.3 2.9 fusion.32
  268.3 3.0 fusion.34
  271.6 2.2 fusion.24
  274.8 1.6 pad_maximum_fusion
  276.4 2.0 copy.153
  279.2 2.5 psum.7
  281.7 7.0 %fusion.6 = bf16[2048,256]{0,1:T(8,128)(2,1)} fusion(bf16[2048,2048]{1,0:T(8,128)(2,1)} %param.28, f32[2048]{0:T(1024)S(1)} %copy-done.19, f32[256]{0:T(256)S(1)} %add_rsqrt_fusion.1, f32[256,2048]{1,0:T(8,128)S(1)} %copy.153, bf16[256,2048]{1,0:T(8,128)(2,1)S(1)} %copy-done.5), kind=kOutput, calls=%fused_computation.24 | convolution fusion | flops 2152726528 | bytes 12592128 | tf_op jit(solution)/shard_map/dot_general | solution.py:205
  288.8 1.3 copy.122
  290.1 36.7 %reduce-scatter.3.cloned.1.call-done = bf16[1024,256]{0,1:T(8,128)(2,1)} async-done(((bf16[2048,256]{0,1:T(8,128)(2,1)}), bf16[1024,256]{0,1:T(8,128)(2,1)}) %reduce-scatter.3.cloned.1.call-update) | async-done | bytes 524304 | tf_op jit(solution)/shard_map/reduce_scatter | solution.py:204
  326.8 2.0 add_convert_fusion.1
  329.6 2.8 tile.20
  332.4 6.9 %all-to-all-start.1 = ((bf16[16,128,1280]{2,1,0:T(8,128)(2,1)}), bf16[16,128,1280]{2,1,0:T(8,128)(2,1)}, u32[]{:S(2)}, u32[]{:S(2)}) async-start(bf16[16,128,1280]{2,1,0:T(8,128)(2,1)} %bitcast.260), calls=%async_computation.2 | async-start | bytes 10485760 | tf_op jit(solution)/shard_map/all_to_all | solution.py:232
  339.5 1.5 fusion.12
  341.0 1.5 fusion.14
  342.5 1.9 collective-permute-start.1
  344.5 55.0 %collective-permute-done.1 = bf16[2048,256]{0,1:T(8,128)(2,1)S(1)} collective-permute-done((bf16[2048,256]{0,1:T(8,128)(2,1)S(1)}, bf16[2048,256]{0,1:T(8,128)(2,1)S(1)}, u32[]{:S(2)}, u32[]{:S(2)}) %collective-permute-start.1) | collective-permute-done | bytes 1048608 | tf_op jit(solution)/shard_map/ppermute | solution.py:44
  399.5 5.7 fusion.2
  405.2 75.9 %all-to-all-done.1 = bf16[16,128,1280]{2,1,0:T(8,128)(2,1)} async-done(((bf16[16,128,1280]{2,1,0:T(8,128)(2,1)}), bf16[16,128,1280]{2,1,0:T(8,128)(2,1)}, u32[]{:S(2)}, u32[]{:S(2)}) %all-to-all-start.1) | async-done | bytes 5242912 | tf_op jit(solution)/shard_map/all_to_all | solution.py:232
  481.1 6.7 %fusion.3 = bf16[1,1280,512]{1,2,0:T(8,128)(2,1)S(1)} fusion(bf16[2048,1280]{1,0:T(8,128)(2,1)} %bitcast.75, bf16[2048,256]{0,1:T(8,128)(2,1)} %copy-done.18, bf16[2048,256]{0,1:T(8,128)(2,1)} %copy-done.7, pred[]{:T(512)S(6)} %eq.5), kind=kOutput, calls=%fused_computation.12 | convolution fusion | flops 2694447104 | bytes 8650753 | tf_op jit(solution)/shard_map/dot_general | solution.py:78
  487.8 10.7 %collective-permute-start.2 = (bf16[2,1280,2]{1,2,0:T(2,128)(2,1)S(1)}, bf16[2,1280,2]{1,2,0:T(2,128)(2,1)S(1)}, u32[]{:S(2)}, u32[]{:S(2)}) collective-permute-start(bf16[2,1280,2]{1,2,0:T(2,128)(2,1)S(1)} %pad_maximum_fusion.4), channel_id=1, source_target_pairs={{0,4},{2,6},{4,8},{6,10},{8,12},{10,14},{12,16},{14,18},{16,20},{1... | collective-permute-start | bytes 30728 | tf_op jit(solution)/shard_map/ppermute | solution.py:18
  498.6 1.1 collective-permute-done.2
  500.2 1.6 fusion
  502.8 30.5 %collective-permute-done.3 = bf16[1280,256]{0,1:T(8,128)(2,1)S(1)} collective-permute-done((bf16[1280,256]{0,1:T(8,128)(2,1)S(1)}, bf16[1280,256]{0,1:T(8,128)(2,1)S(1)}, u32[]{:S(2)}, u32[]{:S(2)}) %collective-permute-start.3) | collective-permute-done | bytes 655392 | tf_op jit(solution)/shard_map/ppermute | solution.py:44
  533.3 59.3 %all-gather.13.cloned.1.call-done = bf16[2560,2048]{1,0:T(8,128)(2,1)} async-done(((bf16[2560,128]{1,0:T(8,128)(2,1)}), bf16[2560,2048]{1,0:T(8,128)(2,1)}) %all-gather.13.cloned.1.call-update) | async-done | bytes 10485776 | tf_op jit(solution)/shard_map/all_gather | solution.py:257
  592.6 7.9 %fusion.7 = bf16[2048,256]{0,1:T(8,128)(2,1)} fusion(bf16[2560,2048]{1,0:T(8,128)(2,1)} %all-gather.13.cloned.1.call-done, bf16[1280,256]{0,1:T(8,128)(2,1)S(1)} %collective-permute-done.3, bf16[1280,256]{0,1:T(8,128)(2,1)S(1)} %get-tuple-element.121, pred[]{:T(512)S(6)} %eq.5), kind=kOutput, calls=%fused_computation.25 | convolution fusion | flops 2690777088 | bytes 12845057 | tf_op jit(solution)/shard_map/dot_general | solution.py:78
  600.5 12.9 %reduce-scatter.5.cloned.1.call-done = bf16[1024,256]{0,1:T(8,128)(2,1)} async-done(((bf16[2048,256]{0,1:T(8,128)(2,1)}), bf16[1024,256]{0,1:T(8,128)(2,1)}) %reduce-scatter.5.cloned.1.call-update) | async-done | bytes 524304 | tf_op jit(solution)/shard_map/reduce_scatter | solution.py:258
  613.4 1.2 add_convert_fusion
  (141 shorter events, 20.6 us)
Async XLA Ops:
  6.5 9.2 %copy-start.8 = (bf16[256,1536]{1,0:T(8,128)(2,1)S(1)}, bf16[256,1536]{1,0:T(8,128)(2,1)}, u32[]{:S(2)}) copy-start(bf16[256,1536]{1,0:T(8,128)(2,1)} %param.21) | copy-start | bytes 2359300
  6.5 9.0 %copy-start.13 = (bf16[4,2048]{1,0:T(4,128)(2,1)S(1)}, bf16[4,2048]{1,0:T(4,128)(2,1)}, u32[]{:S(2)}) copy-start(bf16[4,2048]{1,0:T(4,128)(2,1)} %param.25) | copy-start | bytes 49156
  6.5 9.1 %copy-start.14 = (bf16[4,1536]{1,0:T(4,128)(2,1)S(1)}, bf16[4,1536]{1,0:T(4,128)(2,1)}, u32[]{:S(2)}) copy-start(bf16[4,1536]{1,0:T(4,128)(2,1)} %param.26) | copy-start | bytes 36868
  6.5 264.8 %all-gather.17.cloned.1.call-start = ((), (), s32[]{:S(2)}) async-start(), calls=%async_computation.9 | async-start | bytes 4456448 | tf_op jit(solution)/shard_map/all_gather | solution.py:24
  8.2 8.9 %collective-permute-start = (bf16[3,3584]{1,0:T(4,128)(2,1)S(1)}, bf16[3,3584]{1,0:T(4,128)(2,1)S(1)}, u32[]{:S(2)}, u32[]{:S(2)}) collective-permute-start(bf16[3,3584]{1,0:T(4,128)(2,1)S(1)} %pad_maximum_fusion.3), channel_id=1, source_target_pairs={{0,2},{2,4},{4,6},{6,8},{8,10},{10,12},{12,14},{14,16},{16,18},{18... | collective-permute-start | bytes 64520 | tf_op jit(solution)/shard_map/ppermute | solution.py:18
  15.2 2.2 copy-start.4
  22.5 2.4 copy-start
  26.9 244.4 %all-gather.15.cloned.1.call-start = ((), (), s32[]{:S(2)}) async-start(), calls=%async_computation.8 | async-start | bytes 4456448 | tf_op jit(solution)/shard_map/all_gather | solution.py:24
  27.8 0.7 copy-start.3
  36.6 292.9 %all-to-all-start = ((bf16[16,128,1280]{2,1,0:T(8,128)(2,1)}), bf16[16,128,1280]{2,1,0:T(8,128)(2,1)}, u32[]{:S(2)}, u32[]{:S(2)}) async-start(bf16[16,128,1280]{2,1,0:T(8,128)(2,1)} %bitcast.259), calls=%async_computation.1 | async-start | bytes 10485760 | tf_op jit(solution)/shard_map/all_to_all | solution.py:231
  42.6 4.9 copy-start.12
  42.6 8.5 %copy-start.17 = (f32[32]{0:T(128)S(1)}, f32[32]{0:T(128)}, u32[]{:S(2)}) copy-start(f32[32]{0:T(128)} %param.24) | copy-start | bytes 388
  42.7 284.1 %reduce-scatter.3.cloned.1.call-start = ((), (), s32[]{:S(2)}) async-start(), calls=%async_computation.4 | async-start | bytes 1572864 | tf_op jit(solution)/shard_map/reduce_scatter | solution.py:204
  46.4 4.8 copy-start.6
  257.7 2.4 copy-start.1
  271.6 2.2 copy-start.10
  271.6 2.2 copy-start.11
  276.4 2.0 copy-start.5
  278.5 3.3 copy-start.19
  288.7 40.7 %copy-start.9 = (bf16[128,2560]{1,0:T(8,128)(2,1)S(1)}, bf16[128,2560]{1,0:T(8,128)(2,1)}, u32[]{:S(2)}) copy-start(bf16[128,2560]{1,0:T(8,128)(2,1)} %param.31) | copy-start | bytes 1966084
  288.7 50.7 %all-gather.11.cloned.1.call-start = ((), (), s32[]{:S(2)}) async-start(), calls=%async_computation.5 | async-start | bytes 1572864 | tf_op jit(solution)/shard_map/all_gather | solution.py:213
  328.9 263.7 %all-gather.13.cloned.1.call-start = ((), (), s32[]{:S(2)}) async-start(), calls=%async_computation.6 | async-start | bytes 11141120 | tf_op jit(solution)/shard_map/all_gather | solution.py:257
  332.4 8.6 %copy-start.15 = (f32[2048]{0:T(1024)S(1)}, f32[2048]{0:T(1024)}, u32[]{:S(2)}) copy-start(f32[2048]{0:T(1024)} %param.29) | copy-start | bytes 24580
  332.4 148.7 %all-to-all-start.1 = ((bf16[16,128,1280]{2,1,0:T(8,128)(2,1)}), bf16[16,128,1280]{2,1,0:T(8,128)(2,1)}, u32[]{:S(2)}, u32[]{:S(2)}) async-start(bf16[16,128,1280]{2,1,0:T(8,128)(2,1)} %bitcast.260), calls=%async_computation.2 | async-start | bytes 10485760 | tf_op jit(solution)/shard_map/all_to_all | solution.py:232
  339.4 274.0 %reduce-scatter.5.cloned.1.call-start = ((), (), s32[]{:S(2)}) async-start(), calls=%async_computation.7 | async-start | bytes 1572864 | tf_op jit(solution)/shard_map/reduce_scatter | solution.py:258
  342.5 62.7 %copy-start.7 = (bf16[2048,256]{0,1:T(8,128)(2,1)}, bf16[2048,256]{0,1:T(8,128)(2,1)S(1)}, u32[]{:S(2)}) copy-start(bf16[2048,256]{0,1:T(8,128)(2,1)S(1)} %fusion.14) | copy-start | bytes 3145732
  342.5 56.9 %collective-permute-start.1 = (bf16[2048,256]{0,1:T(8,128)(2,1)S(1)}, bf16[2048,256]{0,1:T(8,128)(2,1)S(1)}, u32[]{:S(2)}, u32[]{:S(2)}) collective-permute-start(bf16[2048,256]{0,1:T(8,128)(2,1)S(1)} %fusion.14), channel_id=1, source_target_pairs={{0,2},{2,0},{4,6},{6,4},{8,10},{10,8},{12,14},{14,12},{16,18},{18,... | collective-permute-start | bytes 3145736 | tf_op jit(solution)/shard_map/ppermute | solution.py:44
  399.5 5.8 copy-start.18
  487.8 10.8 %copy-start.16 = (bf16[2,3,2560]{2,0,1:T(2,128)(2,1)S(1)}, bf16[2,3,2560]{2,0,1:T(2,128)(2,1)}, u32[]{:S(2)}) copy-start(bf16[2,3,2560]{2,0,1:T(2,128)(2,1)} %param.32) | copy-start | bytes 92164
  487.8 11.9 %collective-permute-start.2 = (bf16[2,1280,2]{1,2,0:T(2,128)(2,1)S(1)}, bf16[2,1280,2]{1,2,0:T(2,128)(2,1)S(1)}, u32[]{:S(2)}, u32[]{:S(2)}) collective-permute-start(bf16[2,1280,2]{1,2,0:T(2,128)(2,1)S(1)} %pad_maximum_fusion.4), channel_id=1, source_target_pairs={{0,4},{2,6},{4,8},{6,10},{8,12},{10,14},{12,16},{14,18},{16,20},{1... | collective-permute-start | bytes 30728 | tf_op jit(solution)/shard_map/ppermute | solution.py:18
  502.7 30.6 %collective-permute-start.3 = (bf16[1280,256]{0,1:T(8,128)(2,1)S(1)}, bf16[1280,256]{0,1:T(8,128)(2,1)S(1)}, u32[]{:S(2)}, u32[]{:S(2)}) collective-permute-start(bf16[1280,256]{0,1:T(8,128)(2,1)S(1)} %get-tuple-element.122), channel_id=1, source_target_pairs={{0,2},{2,0},{4,6},{6,4},{8,10},{10,8},{12,14},{14,12},{16,18},{18,... | collective-permute-start | bytes 1966088 | tf_op jit(solution)/shard_map/ppermute | solution.py:44
  592.6 20.9 %copy-start.2 = (bf16[1024,256]{0,1:T(8,128)(2,1)S(1)}, bf16[1024,256]{0,1:T(8,128)(2,1)}, u32[]{:S(2)}) copy-start(bf16[1024,256]{0,1:T(8,128)(2,1)} %add_convert_fusion.1) | copy-start | bytes 1572868
Sparse Core Ops, SparseCore 0:
  27.0 157.4 all-gather.16
  187.2 74.3 all-gather.14
  288.8 37.9 reduce-scatter.2
  329.0 10.1 all-gather.10
  341.7 250.7 all-gather.12
  600.6 12.7 reduce-scatter.4
where the time goes:
time: 632 us; the launch traced here: 623 us
  waiting for transfers between devices  272 us (43%)
  blocking collectives  205 us (32%)
  matrix products  52.4 us (8%)
  starting transfers between devices  30.7 us (5%)
  local copies, waits for them, and re-layouts  26.2 us (4%)
  other arithmetic  21.9 us (3%)
  between operations  14.4 us (2%)
    all_gather x2, blocking collectives, prefix(): lax.all_gather(a.astype(kind), axis)  202 us
    ppermute x2, waiting for transfers between devices, from_partner_2(): lax.ppermute(shard, axis, [(i, i ^ 1 << stride) for i in range(lax.axis_s...  85.5 us
    all_to_all x1, waiting for transfers between devices, local(): lax.all_to_all(up_tiles, 'sp', split_axis=0, concat_axis=0, tiled=True)  75.9 us
    all_gather x1, waiting for transfers between devices, local(): down_whole = lax.all_gather(hidden_down, 'sp', axis=1, tiled=True)  59.3 us
    reduce_scatter x1, waiting for transfers between devices, local(): lax.psum_scatter(lax.dot_general(out_weight, normed, (((0,), (1,)), ((),...  36.7 us
    dot_general x3, matrix products, contract_rows(): lax.dot_general(left, right, (((0,), (0,)), ((), ())), preferred_element_...  20.3 us
    ppermute x2, starting transfers between devices, from_behind(): lax.ppermute(value, axis, [(source, source + steps) for source in range(f...  15.6 us
    reduce_scatter x1, waiting for transfers between devices, local(): lax.psum_scatter(contract_rows(down_whole, hidden).astype(jnp.bfloat16),...  12.9 us
  transfers between devices with their start and end apart: 12, of which 7 were waited for; matrix products, arithmetic and copies ran while one was open for 13% of the time, Pallas kernels for 0%

commit v1 on v0

--- a/solution.py
+++ b/solution.py
@@ -254,7 +254,18 @@
         jnp.concatenate([own_part, from_partner], axis=0),
         jnp.concatenate([from_partner, own_part], axis=0),
     )
-    down_whole = lax.all_gather(hidden_down, "sp", axis=1, tiled=True)
+    w_next = lax.axis_size("sp")
+    s_next = lax.axis_index("sp")
+    opened, formed = (w_next, s_next)
+    down_whole, frame_out = (hidden_down, 1)
+    while frame_out < opened:
+        t_next = lax.ppermute(
+            down_whole, "sp", [(src_i, src_i ^ frame_out) for src_i in range(opened)]
+        )
+        earlier = jnp.concatenate([down_whole, t_next], axis=1)
+        current_arr = jnp.concatenate([t_next, down_whole], axis=1)
+        down_whole = jnp.where(formed & frame_out == 0, earlier, current_arr)
+        frame_out = 2 * frame_out
     hidden_sum = lax.psum_scatter(
         contract_rows(down_whole, hidden).astype(jnp.bfloat16),
         "tp",

time: 632 us -> 733 us (1.16)
  waiting for transfers between devices: 272 us -> 332 us
  starting transfers between devices: 30.7 us -> 53.1 us
  other arithmetic: 21.9 us -> 35.8 us
    ppermute x0 -> x4, waiting for transfers between devices: none -> 279 us  [local(): lax.ppermute(down_whole, 'sp', [(src_i, src_i ^ frame_out) for src_i in r...]
    ppermute x2, waiting for transfers between devices: 85.5 us -> 0.01 us  [from_partner_2(): lax.ppermute(shard, axis, [(i, i ^ 1 << stride) for i in range(lax.axis_s...]
    all_to_all x1, waiting for transfers between devices: 75.9 us -> 0.01 us  [local(): lax.all_to_all(up_tiles, 'sp', split_axis=0, concat_axis=0, tiled=True)]
    all_gather x1 -> x0, waiting for transfers between devices: 59.3 us -> none  [local(): down_whole = lax.all_gather(hidden_down, 'sp', axis=1, tiled=True)]
    reduce_scatter x1, waiting for transfers between devices: 36.7 us -> 0.02 us  [local(): lax.psum_scatter(lax.dot_general(out_weight, normed, (((0,), (1,)), ((),...]
    ppermute x0 -> x4, starting transfers between devices: none -> 28.5 us  [local(): lax.ppermute(down_whole, 'sp', [(src_i, src_i ^ frame_out) for src_i in r...]
    all_gather x1, waiting for transfers between devices: 0.02 us -> 21 us  [local(): merged = lax.all_gather(own_merged, 'tp', axis=0, tiled=True)]
    reduce_scatter x1, waiting for transfers between devices: 12.9 us -> 30.5 us  [local(): lax.psum_scatter(contract_rows(down_whole, hidden).astype(jnp.bfloat16),...]
  transfers between devices with their start and end apart: 12 -> 15, of which waited for: 7 -> 6; matrix products, arithmetic and copies ran while one was open for 13% -> 13% of each run, Pallas kernels for 0% -> 0%
where the time goes in v1:
time: 733 us; the launch traced here: 723 us
  waiting for transfers between devices  332 us (45%)
  blocking collectives  200 us (27%)
  matrix products  59.4 us (8%)
  starting transfers between devices  53.1 us (7%)
  other arithmetic  35.8 us (5%)
  local copies, waits for them, and re-layouts  28.1 us (4%)
  between operations  14.1 us (2%)
    ppermute x4, waiting for transfers between devices, local(): lax.ppermute(down_whole, 'sp', [(src_i, src_i ^ frame_out) for src_i in r...  279 us
    all_gather x2, blocking collectives, prefix(): lax.all_gather(a.astype(kind), axis)  198 us
    reduce_scatter x1, waiting for transfers between devices, local(): lax.psum_scatter(contract_rows(down_whole, hidden).astype(jnp.bfloat16),...  30.5 us
    ppermute x4, starting transfers between devices, local(): lax.ppermute(down_whole, 'sp', [(src_i, src_i ^ frame_out) for src_i in r...  28.5 us
    dot_general x3, matrix products, contract_rows(): lax.dot_general(left, right, (((0,), (0,)), ((), ())), preferred_element_...  26.6 us
    all_gather x1, waiting for transfers between devices, local(): merged = lax.all_gather(own_merged, 'tp', axis=0, tiled=True)  21 us
  transfers between devices with their start and end apart: 15, of which 6 were waited for; matrix products, arithmetic and copies ran while one was open for 13% of the time, Pallas kernels for 0%

profile of v1, /device:TPU:0, one launch (start us, length us, event | category | flops | bytes accessed | tf_op | source)
XLA Modules:
  0.0 723.2 jit_solution(16124550123569989596)
XLA Ops:
  8.2 4.9 collective-permute-start
  19.8 1.8 copy.126
  21.7 1.6 maximum_convert_fusion.1
  23.4 2.4 divide_multiply_fusion.1
  26.4 1.4 fusion.51
  28.9 2.8 tile.8
  31.8 6.0 all-to-all-start
  39.4 1.7 convolution_add_fusion.3
  41.1 2.4 fusion.50
  43.5 1.9 collective-permute-start.1
  45.5 1.7 exp.125
  50.4 2.3 reduce-window.6
  55.6 119.0 %all-gather.4 = bf16[16,4,4]{2,1,0:T(4,128)(2,1)S(1)} all-gather(bf16[1,4,4]{2,1,0:T(4,128)(2,1)S(1)} %get-tuple-element.151), channel_id=2, replica_groups=mesh['sp'=16,'tp'=2] {'sp'}, dimensions={0}, use_global_device_ids=true | all-gather | bytes 544 | tf_op jit(solution)/shard_map/all_gather | solution.py:24
  174.6 79.0 %all-gather.5 = bf16[16,4,4]{2,1,0:T(4,128)(2,1)S(1)} all-gather(bf16[1,4,4]{2,1,0:T(4,128)(2,1)S(1)} %get-tuple-element.150), channel_id=4, replica_groups=mesh['sp'=16,'tp'=2] {'sp'}, dimensions={0}, use_global_device_ids=true | all-gather | bytes 544 | tf_op jit(solution)/shard_map/all_gather | solution.py:24
  259.8 3.0 fusion.43
  262.8 3.0 fusion.45
  265.8 2.9 fusion.39
  268.7 3.0 fusion.41
  271.7 2.9 tile.20
  274.6 4.6 all-to-all-start.1
  280.5 2.1 fusion.29
  283.6 1.5 pad_maximum_fusion
  285.1 2.0 copy.156
  287.9 2.5 psum.7
  290.4 7.0 fusion.14
  297.5 2.1 maximum_select_fusion.9
  299.6 5.7 collective-permute-start.2
  305.3 52.1 %collective-permute-done.2 = bf16[2560,256]{1,0:T(8,128)(2,1)} collective-permute-done((bf16[2560,256]{1,0:T(8,128)(2,1)S(1)}, bf16[2560,256]{1,0:T(8,128)(2,1)}, u32[]{:S(2)}, u32[]{:S(2)}) %collective-permute-start.2) | collective-permute-done | bytes 1310752 | tf_op jit(solution)/shard_map/ppermute | solution.py:262
  357.4 3.0 maximum_select_fusion.3
  360.4 8.8 %collective-permute-start.3 = (bf16[2560,512]{1,0:T(8,128)(2,1)S(1)}, bf16[2560,512]{1,0:T(8,128)(2,1)}, u32[]{:S(2)}, u32[]{:S(2)}) collective-permute-start(bf16[2560,512]{1,0:T(8,128)(2,1)S(1)} %maximum_select_fusion.3), channel_id=1, source_target_pairs={{0,8},{2,10},{4,12},{6,14},{8,0},{10,2},{12,4},{14,6},{16,24},{18,... | collective-permute-start | bytes 7864328 | tf_op jit(solution)/shard_map/ppermute | solution.py:262
  369.2 1.2 copy.125
  370.5 2.0 add_convert_fusion.1
  372.8 21.0 %all-gather.10.cloned.1.call-done = bf16[2048,256]{0,1:T(8,128)(2,1)} async-done(((bf16[1024,256]{0,1:T(8,128)(2,1)}), bf16[2048,256]{0,1:T(8,128)(2,1)}) %all-gather.10.cloned.1.call-update) | async-done | bytes 1048592 | tf_op jit(solution)/shard_map/all_gather | solution.py:213
  393.8 1.5 fusion.19
  395.3 2.5 fusion.21
  397.8 1.7 collective-permute-start.5
  399.6 26.8 %collective-permute-done.3 = bf16[2560,512]{1,0:T(8,128)(2,1)} collective-permute-done((bf16[2560,512]{1,0:T(8,128)(2,1)S(1)}, bf16[2560,512]{1,0:T(8,128)(2,1)}, u32[]{:S(2)}, u32[]{:S(2)}) %collective-permute-start.3) | collective-permute-done | bytes 2621472 | tf_op jit(solution)/shard_map/ppermute | solution.py:262
  426.4 6.9 maximum_select_fusion.2
  433.3 12.1 %collective-permute-start.4 = (bf16[2560,1024]{1,0:T(8,128)(2,1)}, bf16[2560,1024]{1,0:T(8,128)(2,1)}, u32[]{:S(2)}, u32[]{:S(2)}) collective-permute-start(bf16[2560,1024]{1,0:T(8,128)(2,1)} %maximum_select_fusion.2), channel_id=1, source_target_pairs={{0,16},{2,18},{4,20},{6,22},{8,24},{10,26},{12,28},{14,30},{16,0},... | collective-permute-start | bytes 15728648 | tf_op jit(solution)/shard_map/ppermute | solution.py:262
  445.4 6.7 fusion.9
  452.0 6.8 fusion.10
  458.9 3.8 collective-permute-start.6
  462.8 1.3 collective-permute-done.6
  464.6 1.6 fusion.7
  467.1 3.2 collective-permute-start.7
  470.3 200.3 %collective-permute-done.4 = bf16[2560,1024]{1,0:T(8,128)(2,1)} collective-permute-done((bf16[2560,1024]{1,0:T(8,128)(2,1)}, bf16[2560,1024]{1,0:T(8,128)(2,1)}, u32[]{:S(2)}, u32[]{:S(2)}) %collective-permute-start.4) | collective-permute-done | bytes 5242912 | tf_op jit(solution)/shard_map/ppermute | solution.py:262
  670.6 13.2 %fusion.13 = bf16[2048,256]{0,1:T(8,128)(2,1)} fusion(bf16[2560,1024]{1,0:T(8,128)(2,1)} %collective-permute-done.4, bf16[2560,1024]{1,0:T(8,128)(2,1)} %maximum_select_fusion.2, pred[]{:T(512)S(6)} %eq.17, bf16[1280,256]{0,1:T(8,128)(2,1)S(1)} %collective-permute-done.7, bf16[1280,256]{0,1:T(8,128)(2,1)S(1)} %get-tuple-element.121, pred[]{:T(512)S(6)} %eq.21), kind=kOutput, calls=%fused_computation.32 | convolution fusion | flops 2737963008 | bytes 12845058 | tf_op jit(solution)/shard_map/dot_general | solution.py:78
  683.7 30.5 %reduce-scatter.5.cloned.1.call-done = bf16[1024,256]{0,1:T(8,128)(2,1)} async-done(((bf16[2048,256]{0,1:T(8,128)(2,1)}), bf16[1024,256]{0,1:T(8,128)(2,1)}) %reduce-scatter.5.cloned.1.call-update) | async-done | bytes 524304 | tf_op jit(solution)/shard_map/reduce_scatter | solution.py:269
  (145 shorter events, 30.9 us)
Async XLA Ops:
  6.5 10.0 %copy-start.8 = (bf16[256,1536]{1,0:T(8,128)(2,1)S(1)}, bf16[256,1536]{1,0:T(8,128)(2,1)}, u32[]{:S(2)}) copy-start(bf16[256,1536]{1,0:T(8,128)(2,1)} %param.21) | copy-start | bytes 2359300
  6.5 10.0 %copy-start.13 = (bf16[4,1536]{1,0:T(4,128)(2,1)S(1)}, bf16[4,1536]{1,0:T(4,128)(2,1)}, u32[]{:S(2)}) copy-start(bf16[4,1536]{1,0:T(4,128)(2,1)} %param.26) | copy-start | bytes 36868
  6.5 272.7 %all-gather.14.cloned.1.call-start = ((), (), s32[]{:S(2)}) async-start(), calls=%async_computation.8 | async-start | bytes 4456448 | tf_op jit(solution)/shard_map/all_gather | solution.py:24
  8.2 9.8 %collective-permute-start = (bf16[3,3584]{1,0:T(4,128)(2,1)S(1)}, bf16[3,3584]{1,0:T(4,128)(2,1)S(1)}, u32[]{:S(2)}, u32[]{:S(2)}) collective-permute-start(bf16[3,3584]{1,0:T(4,128)(2,1)S(1)} %pad_maximum_fusion.3), channel_id=1, source_target_pairs={{0,2},{2,4},{4,6},{6,8},{8,10},{10,12},{12,14},{14,16},{16,18},{18... | collective-permute-start | bytes 64520 | tf_op jit(solution)/shard_map/ppermute | solution.py:18
  15.2 3.0 copy-start.5
  23.3 2.4 copy-start
  31.8 240.0 %all-to-all-start = ((bf16[16,128,1280]{2,1,0:T(8,128)(2,1)}), bf16[16,128,1280]{2,1,0:T(8,128)(2,1)}, u32[]{:S(2)}, u32[]{:S(2)}) async-start(bf16[16,128,1280]{2,1,0:T(8,128)(2,1)} %bitcast.257), calls=%async_computation.1 | async-start | bytes 10485760 | tf_op jit(solution)/shard_map/all_to_all | solution.py:231
  37.8 241.5 %all-gather.12.cloned.1.call-start = ((), (), s32[]{:S(2)}) async-start(), calls=%async_computation.7 | async-start | bytes 4456448 | tf_op jit(solution)/shard_map/all_gather | solution.py:24
  38.7 0.7 copy-start.4
  43.5 6.8 copy-start.12
  43.5 10.4 %copy-start.16 = (f32[32]{0:T(128)S(1)}, f32[32]{0:T(128)}, u32[]{:S(2)}) copy-start(f32[32]{0:T(128)} %param.24) | copy-start | bytes 388
  43.5 253.9 %collective-permute-start.1 = (bf16[2560,128]{1,0:T(8,128)(2,1)}, bf16[2560,128]{1,0:T(8,128)(2,1)}, u32[]{:S(2)}, u32[]{:S(2)}) collective-permute-start(bf16[2560,128]{1,0:T(8,128)(2,1)} %param.33), channel_id=1, source_target_pairs={{0,2},{2,0},{4,6},{6,4},{8,10},{10,8},{12,14},{14,12},{16,18},{18,... | collective-permute-start | bytes 1966088 | tf_op jit(solution)/shard_map/ppermute | solution.py:262
  49.2 4.8 copy-start.7
  257.4 2.4 copy-start.1
  274.6 177.4 %all-to-all-start.1 = ((bf16[16,128,1280]{2,1,0:T(8,128)(2,1)}), bf16[16,128,1280]{2,1,0:T(8,128)(2,1)}, u32[]{:S(2)}, u32[]{:S(2)}) async-start(bf16[16,128,1280]{2,1,0:T(8,128)(2,1)} %bitcast.256), calls=%async_computation.2 | async-start | bytes 10485760 | tf_op jit(solution)/shard_map/all_to_all | solution.py:232
  279.2 91.3 %reduce-scatter.3.cloned.1.call-start = ((), (), s32[]{:S(2)}) async-start(), calls=%async_computation.4 | async-start | bytes 1572864 | tf_op jit(solution)/shard_map/reduce_scatter | solution.py:204
  279.4 1.0 copy-start.11
  279.6 2.9 copy-start.9
  279.6 2.9 copy-start.10
  285.1 2.0 copy-start.6
  287.2 3.3 copy-start.17
  297.4 96.4 %all-gather.10.cloned.1.call-start = ((), (), s32[]{:S(2)}) async-start(), calls=%async_computation.5 | async-start | bytes 1572864 | tf_op jit(solution)/shard_map/all_gather | solution.py:213
  299.6 5.7 copy-start.2
  299.6 57.8 %collective-permute-start.2 = (bf16[2560,256]{1,0:T(8,128)(2,1)S(1)}, bf16[2560,256]{1,0:T(8,128)(2,1)}, u32[]{:S(2)}, u32[]{:S(2)}) collective-permute-start(bf16[2560,256]{1,0:T(8,128)(2,1)S(1)} %maximum_select_fusion.9), channel_id=1, source_target_pairs={{0,4},{2,6},{4,0},{6,2},{8,12},{10,14},{12,8},{14,10},{16,20},{18,... | collective-permute-start | bytes 3932168 | tf_op jit(solution)/shard_map/ppermute | solution.py:262
  360.4 34.9 %copy-start.14 = (f32[2048]{0:T(1024)S(1)}, f32[2048]{0:T(1024)}, u32[]{:S(2)}) copy-start(f32[2048]{0:T(1024)} %param.29) | copy-start | bytes 24580
  360.4 65.9 %collective-permute-start.3 = (bf16[2560,512]{1,0:T(8,128)(2,1)S(1)}, bf16[2560,512]{1,0:T(8,128)(2,1)}, u32[]{:S(2)}, u32[]{:S(2)}) collective-permute-start(bf16[2560,512]{1,0:T(8,128)(2,1)S(1)} %maximum_select_fusion.3), channel_id=1, source_target_pairs={{0,8},{2,10},{4,12},{6,14},{8,0},{10,2},{12,4},{14,6},{16,24},{18,... | collective-permute-start | bytes 7864328 | tf_op jit(solution)/shard_map/ppermute | solution.py:262
  372.6 341.7 %reduce-scatter.5.cloned.1.call-start = ((), (), s32[]{:S(2)}) async-start(), calls=%async_computation.6 | async-start | bytes 1572864 | tf_op jit(solution)/shard_map/reduce_scatter | solution.py:269
  397.8 47.6 %collective-permute-start.5 = (bf16[2048,256]{0,1:T(8,128)(2,1)}, bf16[2048,256]{0,1:T(8,128)(2,1)}, u32[]{:S(2)}, u32[]{:S(2)}) collective-permute-start(bf16[2048,256]{0,1:T(8,128)(2,1)} %fusion.21), channel_id=1, source_target_pairs={{0,2},{2,0},{4,6},{6,4},{8,10},{10,8},{12,14},{14,12},{16,18},{18,... | collective-permute-start | bytes 3145736 | tf_op jit(solution)/shard_map/ppermute | solution.py:44
  433.3 237.2 %collective-permute-start.4 = (bf16[2560,1024]{1,0:T(8,128)(2,1)}, bf16[2560,1024]{1,0:T(8,128)(2,1)}, u32[]{:S(2)}, u32[]{:S(2)}) collective-permute-start(bf16[2560,1024]{1,0:T(8,128)(2,1)} %maximum_select_fusion.2), channel_id=1, source_target_pairs={{0,16},{2,18},{4,20},{6,22},{8,24},{10,26},{12,28},{14,30},{16,0},... | collective-permute-start | bytes 15728648 | tf_op jit(solution)/shard_map/ppermute | solution.py:262
  458.9 3.9 copy-start.15
  458.9 5.2 collective-permute-start.6
  467.1 203.5 %collective-permute-start.7 = (bf16[1280,256]{0,1:T(8,128)(2,1)S(1)}, bf16[1280,256]{0,1:T(8,128)(2,1)S(1)}, u32[]{:S(2)}, u32[]{:S(2)}) collective-permute-start(bf16[1280,256]{0,1:T(8,128)(2,1)S(1)} %get-tuple-element.122), channel_id=1, source_target_pairs={{0,2},{2,0},{4,6},{6,4},{8,10},{10,8},{12,14},{14,12},{16,18},{18,... | collective-permute-start | bytes 1966088 | tf_op jit(solution)/shard_map/ppermute | solution.py:44
  670.6 43.7 %copy-start.3 = (bf16[1024,256]{0,1:T(8,128)(2,1)S(1)}, bf16[1024,256]{0,1:T(8,128)(2,1)}, u32[]{:S(2)}) copy-start(bf16[1024,256]{0,1:T(8,128)(2,1)} %add_convert_fusion.1) | copy-start | bytes 1572868
Sparse Core Ops, SparseCore 0:
  27.9 160.4 all-gather.13
  191.1 81.1 all-gather.11
  297.5 43.0 reduce-scatter.2
  372.7 21.0 all-gather.9
  683.9 30.3 reduce-scatter.4
